TPU v7x, 512 devices: a 4x2x32 block of a 4x8x32 slice. The times are simulated.
512 devices in a mesh: grp: 2 (over y), sp: 32 (over z), tp: 8 (over x, core).
Axes of the slice: x: 4, y: 2, z: 32, core: 2. Of those that a mesh axis runs over, the one named last changes fastest.
The devices are a block of a 4x8x32 slice.
Arguments:
- inputs: bfloat16 [16384, 2048], P(('grp', 'sp')), parts along dimension 0, may hold values from -6 to 6
- norm_gain: float32 [2048], replicated, may hold values from 0.1 to 1.9
- da_query_weight: bfloat16 [2048, 1024], P('sp', 'tp'), may hold values from -0.125 to 0.125
- da_key_weight: bfloat16 [2048, 1024], P('sp', 'tp'), may hold values from -0.125 to 0.125
- da_value_weight: bfloat16 [2048, 1024], P('sp', 'tp'), may hold values from -0.125 to 0.125
- sw_query_weight: bfloat16 [2048, 1024], P('sp', 'tp'), may hold values from -0.125 to 0.125
- sw_key_weight: bfloat16 [2048, 512], P('sp', 'tp'), may hold values from -0.125 to 0.125
- sw_value_weight: bfloat16 [2048, 512], P('sp', 'tp'), may hold values from -0.125 to 0.125
- da_query_gain: float32 [64], replicated, may hold values from 0.6 to 30
- da_key_gain: float32 [64], replicated, may hold values from 0.6 to 30
- sw_query_gain: float32 [64], replicated, may hold values from 0.6 to 30
- sw_key_gain: float32 [64], replicated, may hold values from 0.6 to 30
- mix_lambda: float32 [8], P('tp'), may hold values from 0.3 to 0.8
- head_gain: float32 [128], replicated, may hold values from 0.1 to 1.9
- sink_logit: float32 [16], P('tp'), may hold values from 0 to 8
- da_out_weight: bfloat16 [1024, 2048], P('tp'), may hold values from -0.1875 to 0.1875
- sw_out_weight: bfloat16 [1024, 2048], P('tp'), may hold values from -0.1875 to 0.1875
Outputs:
- mixed: bfloat16 [16384, 2048], P(('grp', 'sp')), parts along dimension 0
There are 2 independent parts, one for each index of `grp`. A program takes and returns all parts, laid end to end along the dimension named above; an argument that names none is the same for every part. Nothing has to cross between parts.
All inputs are finite; a program needn't handle non-finite values.
Results may differ from a plain program's by a relative error of at most 0.014.
The roundings to bfloat16 on the way count: a program that leaves them out, or rounds other values in their place, can miss the bound.
Values may be sent and summed in bfloat16 or wider, within the bound.
No kernel may reach another device: no remote copies, remote signals or barrier semaphores. Data moves between devices by JAX's collectives and lax.ppermute only.
A program may use at most 64 MiB of HBM per device.

v0:
```python
import jax
import jax.numpy as jnp
from jax import lax
from jax.sharding import PartitionSpec as P

HD = 64
WINDOW = 128


def in_one_piece(arrays, axis, dim, along):
    columns = [a.reshape(*a.shape[:along], -1) for a in arrays]
    both = jnp.concatenate(columns, axis=along)
    whole, at, outs = (lax.all_gather(both, axis, axis=dim, tiled=True), 0, [])
    for a, column in zip(arrays, columns):
        piece = whole[..., at : at + column.shape[along]]
        outs.append(piece.reshape(*piece.shape[:along], *a.shape[along:]))
        at += column.shape[along]
    return tuple(outs)


def sent_together(arrays, axis, dim, along):
    both = jnp.concatenate(arrays, axis=along)
    whole, at, outs = (lax.all_gather(both, axis, axis=dim, tiled=True), 0, [])
    for a in arrays:
        outs.append(lax.slice_in_dim(whole, at, at + a.shape[along], axis=along))
        at += a.shape[along]
    return tuple(outs)


def shifted(value, axis, steps):
    count = lax.axis_size(axis)
    first, last = (max(0, -steps), min(count, count - steps))
    return lax.ppermute(value, axis, [(source, source + steps) for source in range(first, last)])


def over_pieces(shard, axis):
    return lax.all_gather(shard, axis).astype(jnp.float32).sum(0)


def rms_norm(values, gain):
    return values * lax.rsqrt(jnp.mean(values * values, axis=-1, keepdims=True) + 1e-06) * gain


def absorb(state, queries, places, keys, values, key_places):
    top, total, summed = state
    scores = jnp.einsum(
        "qhmd,khmd->hmqk", queries, keys, preferred_element_type=jnp.float32
    ) * HD ** (-0.5)
    scores = jnp.where(key_places[None, :] <= places[:, None], scores, -jnp.inf)
    new_top = jnp.maximum(top, jnp.max(scores, axis=-1))
    weights = jnp.exp(scores - new_top[..., None])
    total = jnp.sum(weights, axis=-1)
    summed = jnp.einsum(
        "hmqk,khe->hmqe", weights.astype(jnp.bfloat16), values, preferred_element_type=jnp.float32
    )
    return (new_top, total, summed)


def keep(state, queries, places, keys, values, key_places):
    return state


def diff_attention(queries, places, da_key, da_value, mix_lambda, head_gain):
    rows = queries.shape[0]
    heads = queries.shape[1]
    half = rows // 2
    fresh = (
        jnp.full((heads, 2, half), -1e30, jnp.float32),
        jnp.zeros((heads, 2, half), jnp.float32),
        jnp.zeros((heads, 2, half, 2 * HD), jnp.float32),
    )
    states = (fresh, fresh)
    start = jnp.int32(0)
    keys, values = in_one_piece((da_key, da_value), "sp", 0, 2)
    key_places = jnp.arange(keys.shape[0], dtype=jnp.int32)
    updated = []
    for section in range(2):
        own_rows = queries[section * half : (section + 1) * half]
        own_places = places[section * half : (section + 1) * half]
        updated.append(
            lax.cond(
                start <= jnp.max(own_places),
                absorb,
                keep,
                states[section],
                own_rows,
                own_places,
                keys,
                values,
                key_places,
            )
        )
    states = tuple(updated)
    blended = []
    for top, total, summed in states:
        maps = summed / total[..., None]
        blended.append(maps[:, 0] - mix_lambda[:, None, None] * maps[:, 1])
    blend = jnp.transpose(jnp.concatenate(blended, axis=1), (1, 0, 2))
    return rms_norm(blend, head_gain).astype(jnp.bfloat16).reshape(rows, heads * 2 * HD)


def window_attention(sw_query, sw_key, sw_value, earlier_key, earlier_value, sink_logit, first):
    rows = sw_query.shape[0]
    sw_heads = sw_query.shape[1]
    kv_heads = sw_key.shape[1]
    groups = sw_heads // kv_heads
    count = rows // WINDOW

    def band(own, earlier_tile):
        tiles = own.reshape(count, WINDOW, kv_heads, HD)
        earlier = jnp.concatenate([earlier_tile[None], tiles[:-1]], axis=0)
        return jnp.concatenate([earlier, tiles], axis=1)

    key_band = band(sw_key, earlier_key)
    value_band = band(sw_value, earlier_value)
    query_tiles = sw_query.reshape(count, WINDOW, kv_heads, groups, HD)
    scores = jnp.einsum(
        "nqhgd,nkhd->nhgqk", query_tiles, key_band, preferred_element_type=jnp.float32
    ) * HD ** (-0.5)
    lag = WINDOW + jnp.arange(WINDOW)[:, None] - jnp.arange(2 * WINDOW)[None, :]
    key_places = (
        first + jnp.arange(count)[:, None] * WINDOW - WINDOW + jnp.arange(2 * WINDOW)[None, :]
    )
    valid = ((lag >= 0) & (lag < WINDOW))[None] & (key_places >= 0)[:, None, :]
    scores = jnp.where(valid[:, None, None], scores, -jnp.inf)
    sink = sink_logit.reshape(kv_heads, groups)[None, :, :, None]
    top = jnp.maximum(jnp.max(scores, axis=-1), sink)
    weights = jnp.exp(scores - top[..., None])
    total = jnp.sum(weights, axis=-1) + jnp.exp(sink - top)
    summed = jnp.einsum(
        "nhgqk,nkhd->nqhgd",
        weights.astype(jnp.bfloat16),
        value_band,
        preferred_element_type=jnp.float32,
    )
    return (
        (summed / jnp.transpose(total, (0, 3, 1, 2))[..., None])
        .astype(jnp.bfloat16)
        .reshape(rows, sw_heads * HD)
    )


def on_device(
    inputs,
    norm_gain,
    da_query_weight,
    da_key_weight,
    da_value_weight,
    sw_query_weight,
    sw_key_weight,
    sw_value_weight,
    da_query_gain,
    da_key_gain,
    sw_query_gain,
    sw_key_gain,
    mix_lambda,
    head_gain,
    sink_logit,
    da_out_weight,
    sw_out_weight,
):
    rows = inputs.shape[0]
    normed = rms_norm(inputs.astype(jnp.float32), norm_gain).astype(jnp.bfloat16)
    pieces = sent_together(
        (
            da_query_weight,
            da_key_weight,
            da_value_weight,
            sw_query_weight,
            sw_key_weight,
            sw_value_weight,
        ),
        "sp",
        0,
        1,
    )
    projected = tuple(
        (jnp.dot(normed, piece, preferred_element_type=jnp.float32) for piece in pieces)
    )
    da_heads = da_query_weight.shape[1] // (2 * HD)
    sw_heads = sw_query_weight.shape[1] // HD
    kv_heads = sw_key_weight.shape[1] // HD
    da_query = rms_norm(projected[0].reshape(rows, da_heads, 2, HD), da_query_gain).astype(
        jnp.bfloat16
    )
    da_key = rms_norm(projected[1].reshape(rows, da_heads, 2, HD), da_key_gain).astype(jnp.bfloat16)
    da_value = projected[2].astype(jnp.bfloat16).reshape(rows, da_heads, 2 * HD)
    sw_query = rms_norm(projected[3].reshape(rows, sw_heads, HD), sw_query_gain).astype(
        jnp.bfloat16
    )
    sw_key = rms_norm(projected[4].reshape(rows, kv_heads, HD), sw_key_gain).astype(jnp.bfloat16)
    sw_value = projected[5].astype(jnp.bfloat16).reshape(rows, kv_heads, HD)
    place = lax.axis_index("sp")
    first = place * rows
    earlier_key, earlier_value = shifted(
        (sw_key[rows - WINDOW :], sw_value[rows - WINDOW :]), "sp", 1
    )
    sw_rows = window_attention(
        sw_query, sw_key, sw_value, earlier_key, earlier_value, sink_logit, first
    )
    places = first + jnp.arange(rows, dtype=jnp.int32)
    da_rows = diff_attention(da_query, places, da_key, da_value, mix_lambda, head_gain)
    partial_value = jnp.dot(da_rows, da_out_weight, preferred_element_type=jnp.float32) + jnp.dot(
        sw_rows, sw_out_weight, preferred_element_type=jnp.float32
    )
    return (
        over_pieces(partial_value.astype(jnp.bfloat16), "tp")
        .astype(jnp.float32)
        .astype(jnp.bfloat16)
    )


def solution(mesh):
    return jax.shard_map(
        on_device,
        mesh=mesh,
        in_specs=(
            P(("grp", "sp"), None),
            P(),
            P("sp", "tp"),
            P("sp", "tp"),
            P("sp", "tp"),
            P("sp", "tp"),
            P("sp", "tp"),
            P("sp", "tp"),
            P(),
            P(),
            P(),
            P(),
            P("tp"),
            P(),
            P("tp"),
            P("tp", None),
            P("tp", None),
        ),
        out_specs=P(("grp", "sp"), None),
        check_vma=False,
    )
```

profile of v0, /device:TPU:33, one launch (start us, length us, event | category | flops | bytes accessed | tf_op | source)
XLA Modules:
  0.0 412.7 jit_solution(8367161722875989220)
XLA Ops:
  6.6 1.6 concatenate.21
  9.0 1.5 fusion.31
  10.5 1.5 fusion.33
  12.1 140.3 %all-gather.5.cloned.1.call-done = bf16[2048,640]{1,0:T(8,128)(2,1)} async-done(((bf16[64,640]{1,0:T(8,128)(2,1)}), bf16[2048,640]{1,0:T(8,128)(2,1)}) %all-gather.5.cloned.1.call-update) | async-done | bytes 2621456 | tf_op jit(solution)/shard_map/all_gather | solution.py:23
  152.4 1.5 bitcast_reduce_fusion.1
  154.0 1.5 fusion.36
  159.3 1.5 multiply_reduce_fusion.2
  160.9 1.5 collective-permute-start.1
  162.4 1.7 convolution_convert_fusion.1
  164.1 2.9 collective-permute-start
  167.1 1.5 fusion.47
  168.7 1.5 bitcast_reduce_fusion
  171.3 128.1 %all-gather.7.cloned.1.call-done = bf16[8192,1,256]{0,2,1:T(8,128)(2,1)} async-done(((bf16[256,1,256]{0,2,1:T(8,128)(2,1)}), bf16[8192,1,256]{0,2,1:T(8,128)(2,1)}) %all-gather.7.cloned.1.call-update) | async-done | bytes 4194320 | tf_op jit(solution)/shard_map/all_gather | solution.py:13
  299.5 3.9 fusion.93
  303.4 7.0 %conditional.2 = (f32[1,2,128]{2,1,0:T(2,128)S(1)}, f32[1,2,128,128]{3,2,1,0:T(8,128)S(1)}) conditional(s32[]{:T(128)} %convert_element_type.72, () %tuple.21, (s32[8192]{0:T(1024)S(1)}, s32[128]{0:T(128)S(1)}, bf16[256,1,2,64]{0,3,2,1:T(8,128)(2,1)S(1)}, bf16[8192,1,2,64]{0,3,2,1:T(8,128)(2,1)}, bf16[8192,1,128]{0,2,1:T(8,128)(2,1)S(1)}) %tuple.22), branch_computations={%region_4.0_spmd, %region_5.8_spmd} | conditional | flops 821034752 | bytes 31660560 | solution.py:81
  304.0 3.6 fusion.91
  307.6 1.4 fusion.8
  309.0 1.3 fusion.2
  310.5 7.2 %conditional.3 = (f32[1,2,128]{2,1,0:T(2,128)S(1)}, f32[1,2,128,128]{3,2,1,0:T(8,128)S(1)}) conditional(s32[]{:T(128)} %convert_element_type.79, () %tuple.23, (s32[8192]{0:T(1024)S(1)}, s32[128]{0:T(128)S(1)}, bf16[256,1,2,64]{0,3,2,1:T(8,128)(2,1)S(1)}, bf16[8192,1,2,64]{0,3,2,1:T(8,128)(2,1)}, bf16[8192,1,128]{0,2,1:T(8,128)(2,1)S(1)}) %tuple.24), branch_computations={%region_9.10_spmd, %region_10.13_spmd} | conditional | flops 821034752 | bytes 31660560 | solution.py:81
  311.4 3.6 fusion.92
  315.0 1.4 fusion.23
  318.8 1.4 fusion.30
  320.3 79.5 %all-gather.9.cloned.1.call-done = bf16[2048,2048]{1,0:T(8,128)(2,1)} async-done(((bf16[256,2048]{1,0:T(8,128)(2,1)}), bf16[2048,2048]{1,0:T(8,128)(2,1)}) %all-gather.9.cloned.1.call-update) | async-done | bytes 8388624 | tf_op jit(solution)/shard_map/all_gather | solution.py:37
  399.7 6.4 %reduce_sum.107 = bf16[256,2048]{1,0:T(8,128)(2,1)} reduce(bf16[8,256,2048]{2,1,0:T(8,128)(2,1)} %bitcast.152, bf16[]{:T(256)} %constant.68.clone.1), dimensions={0}, to_apply=%region_18.19 | reduce | flops 3670016 | bytes 9437186 | tf_op jit(solution)/shard_map/reduce_sum | solution.py:37
  (67 shorter events, 7.8 us)
Async XLA Ops:
  6.5 311.5 %copy-start = (bf16[128,2048]{1,0:T(8,128)(2,1)S(1)}, bf16[128,2048]{1,0:T(8,128)(2,1)}, u32[]{:S(2)}) copy-start(bf16[128,2048]{1,0:T(8,128)(2,1)} %param.36) | copy-start | bytes 1572868
  6.6 145.8 %all-gather.5.cloned.1.call-start = ((), (), s32[]{:S(2)}) async-start(), calls=%async_computation | async-start | bytes 2703360 | tf_op jit(solution)/shard_map/all_gather | solution.py:23
  8.2 291.3 %all-gather.7.cloned.1.call-start = ((), (), s32[]{:S(2)}) async-start(), calls=%async_computation.1 | async-start | bytes 4325376 | tf_op jit(solution)/shard_map/all_gather | solution.py:13
  12.1 148.8 %copy-start.3 = (f32[64]{0:T(128)S(1)}, f32[64]{0:T(128)}, u32[]{:S(2)}) copy-start(f32[64]{0:T(128)} %param.32) | copy-start | bytes 772
  156.3 243.4 %all-gather.9.cloned.1.call-start = ((), (), s32[]{:S(2)}) async-start(), calls=%async_computation.2 | async-start | bytes 9437184 | tf_op jit(solution)/shard_map/all_gather | solution.py:37
  159.3 9.4 %copy-start.4 = (f32[64]{0:T(128)S(1)}, f32[64]{0:T(128)}, u32[]{:S(2)}) copy-start(f32[64]{0:T(128)} %param.29) | copy-start | bytes 772
  160.9 9.5 %copy-start.6 = (f32[64]{0:T(128)S(1)}, f32[64]{0:T(128)}, u32[]{:S(2)}) copy-start(f32[64]{0:T(128)} %param.31) | copy-start | bytes 772
  160.9 9.5 %collective-permute-start.1 = (bf16[128,1,64]{0,2,1:T(8,128)(2,1)S(1)}, bf16[128,1,64]{0,2,1:T(8,128)(2,1)S(1)}, u32[]{:S(2)}, u32[]{:S(2)}) collective-permute-start(bf16[128,1,64]{0,2,1:T(8,128)(2,1)S(1)} %get-tuple-element.75), channel_id=1, source_target_pairs={{0,8},{8,16},{16,24},{24,32},{32,40},{40,48},{48,56},{56,64},{64,7... | collective-permute-start | bytes 49160 | tf_op jit(solution)/shard_map/ppermute | solution.py:33
  164.1 6.7 %copy-start.2 = (f32[2]{0:T(128)S(1)}, f32[2]{0:T(128)}, u32[]{:S(2)}) copy-start(f32[2]{0:T(128)} %param.35) | copy-start | bytes 28
  164.1 6.9 %collective-permute-start = (bf16[128,1,64]{0,2,1:T(8,128)(2,1)S(1)}, bf16[128,1,64]{0,2,1:T(8,128)(2,1)S(1)}, u32[]{:S(2)}, u32[]{:S(2)}) collective-permute-start(bf16[128,1,64]{0,2,1:T(8,128)(2,1)S(1)} %get-tuple-element.73), channel_id=1, source_target_pairs={{0,8},{8,16},{16,24},{24,32},{32,40},{40,48},{48,56},{56,64},{64,7... | collective-permute-start | bytes 49160 | tf_op jit(solution)/shard_map/ppermute | solution.py:33
  310.5 7.5 %copy-start.5 = (f32[128]{0:T(128)S(1)}, f32[128]{0:T(128)}, u32[]{:S(2)}) copy-start(f32[128]{0:T(128)} %param.34) | copy-start | bytes 1540
  317.7 1.0 copy-start.1
Sparse Core Ops, SparseCore 0:
  9.4 142.8 all-gather.4
  156.4 143.0 all-gather.6
  320.4 79.2 all-gather.8
where the time goes:
time: 413 us
  waiting for transfers between devices  348 us (84%)
  matrix products  21.7 us (5%)
  other arithmetic  16 us (4%)
  between operations  15.4 us (4%)
  local copies, waits for them, and re-layouts  6.75 us (2%)
  starting transfers between devices  4.53 us (1%)
    all_gather x1, waiting for transfers between devices, sent_together(): whole, at, outs = (lax.all_gather(both, axis, axis=dim, tiled=True), 0, [])  140 us
    all_gather x1, waiting for transfers between devices, in_one_piece(): whole, at, outs = (lax.all_gather(both, axis, axis=dim, tiled=True), 0, [])  128 us
    all_gather x1, waiting for transfers between devices, over_pieces(): return lax.all_gather(shard, axis).astype(jnp.float32).sum(0)  79.5 us
    dot_general x6, matrix products, on_device(): jnp.dot(normed, piece, preferred_element_type=jnp.float32)  9.32 us
  transfers between devices with their start and end apart: 5, of which 3 were waited for; matrix products, arithmetic and copies ran while one was open for 3% of the time, Pallas kernels for 0%

commit v1 on v0

v1 whole, which is shorter than its diff:
```python
import functools

import jax
import jax.numpy as jnp
from jax import lax
from jax.experimental import pallas as pl
from jax.experimental.pallas import tpu as pltpu
from jax.sharding import PartitionSpec as P

HD = 64
WINDOW = 128
EPS = 1e-06
CUBE = 4
SPARE = 8
STAT_ROWS = 16
NEG = -1e30
MIB = 1024 * 1024


def dot(a, b):
    return lax.dot_general(a, b, (((1,), (0,)), ((), ())), preferred_element_type=jnp.float32)


def dot_t(a, b):
    return lax.dot_general(a, b, (((1,), (1,)), ((), ())), preferred_element_type=jnp.float32)


def half_norm(values, gain):
    low = lax.broadcasted_iota(jnp.int32, values.shape, 1) < HD
    squares = values * values
    first = jnp.sum(jnp.where(low, squares, 0.0), axis=-1, keepdims=True) / HD
    second = jnp.sum(jnp.where(low, 0.0, squares), axis=-1, keepdims=True) / HD
    scale = jnp.where(low, lax.rsqrt(first + EPS), lax.rsqrt(second + EPS))
    return values * scale * gain


def project(place_ref, blocks_ref, pieces, width, rows):
    member = lax.rem(place_ref[0], CUBE)
    total = jnp.zeros((rows, width), jnp.float32)
    for slot, piece in enumerate(pieces):
        source = lax.rem(member - slot + CUBE, CUBE)
        total += dot(blocks_ref[source, :rows, :], piece[...])
    return total


def da_project_kernel(rows, place_ref, blocks_ref, w0, w1, w2, w3, gain_q, gain_k, q_ref, kv_ref, spare_ref):
    everything = blocks_ref.shape[1]
    total = project(place_ref, blocks_ref, (w0, w1, w2, w3), 6 * HD, everything)
    key = half_norm(total[:, : 2 * HD], gain_k[...]).astype(jnp.bfloat16)
    value = total[:, 2 * HD : 4 * HD].astype(jnp.bfloat16)
    q_ref[...] = half_norm(total[:rows, 4 * HD :], gain_q[...]).astype(jnp.bfloat16)
    sent = rows - SPARE
    kv_ref[:, : 2 * HD] = key[:sent]
    kv_ref[:, 2 * HD :] = value[:sent]
    spare_ref[:, : 2 * HD] = key[rows:]
    spare_ref[:, 2 * HD :] = value[rows:]


def sw_project_kernel(rows, place_ref, blocks_ref, w0, w1, w2, w3, gain_q, gain_k, q_ref, kv_ref):
    total = project(place_ref, blocks_ref, (w0, w1, w2, w3), 4 * HD, rows)
    q_ref[...] = half_norm(total[:, : 2 * HD], gain_q[...]).astype(jnp.bfloat16)
    kv = total[:, 2 * HD :]
    low = lax.broadcasted_iota(jnp.int32, kv.shape, 1) < HD
    kv_ref[...] = jnp.where(low, half_norm(kv, gain_k[...]), kv).astype(jnp.bfloat16)


def da_attend_kernel(first_ref, q_ref, kv_ref, places_ref, out_ref):
    rows = q_ref.shape[1]
    first = first_ref[pl.program_id(0)]
    query = q_ref[0]
    key = kv_ref[:, : 2 * HD]
    value = kv_ref[:, 2 * HD :]
    lane = lax.broadcasted_iota(jnp.int32, (rows, 2 * HD), 1)
    own = first + lax.broadcasted_iota(jnp.int32, (rows, 1), 0)
    valid = places_ref[...] <= own
    stats = jnp.zeros((rows, 2 * HD), jnp.float32)
    for m in range(2):
        mine = (lane < HD) if m == 0 else (lane >= HD)
        scores = dot_t(jnp.where(mine, query, jnp.zeros_like(query)), key) * HD ** (-0.5)
        scores = jnp.where(valid, scores, NEG)
        top = jnp.max(scores, axis=-1, keepdims=True)
        weights = jnp.exp(scores - top)
        total = jnp.sum(weights, axis=-1, keepdims=True)
        summed = dot(weights.astype(jnp.bfloat16), value)
        out_ref[0, :rows, m * 2 * HD : (m + 1) * 2 * HD] = (summed / total).astype(jnp.bfloat16)
        rest = top + jnp.log(total)
        for part in range(3):
            head = rest.astype(jnp.bfloat16).astype(jnp.float32)
            stats = jnp.where(lane == 3 * m + part, head, stats)
            rest = rest - head
    out_ref[0, rows:, :] = jnp.transpose(stats)[:STAT_ROWS].astype(jnp.bfloat16)


def merge_kernel(lambda_ref, a0, a1, a2, a3, gain_ref, out_ref):
    rows = out_ref.shape[0]
    pieces = (a0, a1, a2, a3)
    shares = []
    for m in range(2):
        logs = []
        for piece in pieces:
            stat = piece[rows:, :].astype(jnp.float32)
            logs.append(stat[3 * m : 3 * m + 1] + stat[3 * m + 1 : 3 * m + 2] + stat[3 * m + 2 : 3 * m + 3])
        top = functools.reduce(jnp.maximum, logs)
        weights = [jnp.exp(log - top) for log in logs]
        total = functools.reduce(jnp.add, weights)
        shares.extend(weight / total for weight in weights)
    table = jnp.concatenate(shares + [jnp.zeros((2 * HD - len(shares), rows), jnp.float32)], axis=0)
    columns = jnp.transpose(table)
    maps = []
    for m in range(2):
        summed = jnp.zeros((rows, 2 * HD), jnp.float32)
        for i, piece in enumerate(pieces):
            at = len(pieces) * m + i
            summed += columns[:, at : at + 1] * piece[:rows, m * 2 * HD : (m + 1) * 2 * HD].astype(jnp.float32)
        maps.append(summed)
    blend = maps[0] - lambda_ref[0] * maps[1]
    scale = lax.rsqrt(jnp.mean(blend * blend, axis=-1, keepdims=True) + EPS)
    out_ref[...] = (blend * scale * gain_ref[...]).astype(jnp.bfloat16)


def sw_attend_kernel(place_ref, sink_ref, q_ref, before_ref, own_ref, out_ref):
    rows = q_ref.shape[0]
    kv = jnp.concatenate([before_ref[...], own_ref[...]], axis=0)
    query = q_ref[...].astype(jnp.float32)
    low = lax.broadcasted_iota(jnp.int32, query.shape, 1) < HD
    shape = (rows, rows + WINDOW)
    column = lax.broadcasted_iota(jnp.int32, shape, 1)
    lag = WINDOW + lax.broadcasted_iota(jnp.int32, shape, 0) - column
    earliest = jnp.where(place_ref[0] == 0, WINDOW, 0)
    valid = (lag >= 0) & (lag < WINDOW) & (column >= earliest)
    outs = []
    for j in range(2):
        mine = query if j == 0 else pltpu.roll(query, HD, 1)
        scores = dot_t(jnp.where(low, mine, 0.0).astype(jnp.bfloat16), kv) * HD ** (-0.5)
        scores = jnp.where(valid, scores, NEG)
        sink = sink_ref[j]
        top = jnp.maximum(jnp.max(scores, axis=-1, keepdims=True), sink)
        weights = jnp.exp(scores - top)
        total = jnp.sum(weights, axis=-1, keepdims=True) + jnp.exp(sink - top)
        outs.append(dot(weights.astype(jnp.bfloat16), kv) / total)
    out_ref[...] = jnp.where(low, pltpu.roll(outs[0], HD, 1), outs[1]).astype(jnp.bfloat16)


def mix_kernel(core_ref, same_ref, other_ref, w_ref, out_ref):
    total = jnp.zeros(out_ref.shape, jnp.float32)
    core = core_ref[0]
    for chip in range(same_ref.shape[0]):
        for rows_ref, index in ((same_ref, 2 * chip + core), (other_ref, 2 * chip + 1 - core)):
            total += dot(rows_ref[chip], w_ref[index]).astype(jnp.bfloat16).astype(jnp.float32)
    out_ref[...] = total.astype(jnp.bfloat16)


SMEM = pl.BlockSpec(memory_space=pltpu.SMEM)
VMEM = pl.BlockSpec(memory_space=pltpu.VMEM)


def call(kernel, out_shape, specs, args, name, flops):
    return pl.pallas_call(
        kernel,
        out_shape=out_shape,
        in_specs=specs,
        name=name,
        cost_estimate=pl.CostEstimate(flops=flops, bytes_accessed=4 * MIB, transcendentals=0),
        compiler_params=pltpu.CompilerParams(vmem_limit_bytes=48 * MIB),
    )(*args)


def shape_of(*dims):
    return jax.ShapeDtypeStruct(dims, jnp.bfloat16)


def twice(gain):
    return jnp.concatenate([gain, gain])[None]


def in_cube(value, count, steps):
    pairs = [(z, z // CUBE * CUBE + (z + steps) % CUBE) for z in range(count)]
    return lax.ppermute(value, "sp", pairs)


def on_device(
    inputs,
    norm_gain,
    da_query_weight,
    da_key_weight,
    da_value_weight,
    sw_query_weight,
    sw_key_weight,
    sw_value_weight,
    da_query_gain,
    da_key_gain,
    sw_query_gain,
    sw_key_gain,
    mix_lambda,
    head_gain,
    sink_logit,
    da_out_weight,
    sw_out_weight,
):
    rows, width = inputs.shape
    depth = da_query_weight.shape[0]
    count = lax.axis_size("sp")
    groups = lax.axis_size("tp")
    cubes = count // CUBE
    place = lax.axis_index("sp").astype(jnp.int32)
    member = lax.rem(place, CUBE)
    place_arg = place.reshape(1)
    strided = [list(range(r, count, CUBE)) for r in range(CUBE)]

    out_weights = lax.all_gather(
        jnp.concatenate([da_out_weight, sw_out_weight], axis=0), "tp", axis=0, tiled=False
    )

    da_cols = 6 * HD
    sw_cols = 4 * HD
    shard = jnp.concatenate(
        [
            da_key_weight,
            da_value_weight,
            da_query_weight,
            sw_query_weight,
            sw_key_weight,
            sw_value_weight,
            inputs[rows - SPARE :].reshape(depth, SPARE * width // depth),
        ],
        axis=1,
    )
    gathered = lax.all_gather(shard, "sp", axis=0, tiled=True, axis_index_groups=strided)
    da_piece = gathered[:, :da_cols]
    sw_piece = gathered[:, da_cols : da_cols + sw_cols]
    spare_rows = gathered[:, da_cols + sw_cols :].reshape(cubes * SPARE, width)
    da_pieces = [da_piece] + [in_cube(da_piece, count, k) for k in range(1, CUBE)]

    everything = jnp.concatenate([inputs, spare_rows], axis=0).astype(jnp.float32)
    mean = jnp.mean(everything * everything, axis=-1, keepdims=True)
    normed = (everything * lax.rsqrt(mean + EPS) * norm_gain).astype(jnp.bfloat16)
    total_rows = rows + cubes * SPARE
    blocks = (
        normed.reshape(total_rows, cubes, CUBE, depth)
        .transpose(2, 0, 1, 3)
        .reshape(CUBE, total_rows, cubes * depth)
    )

    query, kv_sent, kv_spare = call(
        functools.partial(da_project_kernel, rows),
        (
            shape_of(rows, 2 * HD),
            shape_of(rows - SPARE, 4 * HD),
            shape_of(cubes * SPARE, 4 * HD),
        ),
        [SMEM] + [VMEM] * 7,
        (place_arg, blocks, *da_pieces, twice(da_query_gain), twice(da_key_gain)),
        "da_project",
        2 * total_rows * width * da_cols,
    )
    queries = jnp.stack([query] + [in_cube(query, count, k) for k in range(1, CUBE)])
    kv_far = lax.all_gather(kv_sent, "sp", axis=0, tiled=True, axis_index_groups=strided)
    kv = jnp.concatenate([kv_far, kv_spare], axis=0)

    cube = jnp.arange(cubes, dtype=jnp.int32)[:, None] * (CUBE * rows)
    far_places = (cube + jnp.arange(rows - SPARE, dtype=jnp.int32)[None]).reshape(-1)
    spare_places = (cube + jnp.arange(rows - SPARE, rows, dtype=jnp.int32)[None]).reshape(-1)
    places = (jnp.concatenate([far_places, spare_places]) + member * rows)[None]
    sources = lax.rem(member - jnp.arange(CUBE, dtype=jnp.int32) + CUBE, CUBE)
    firsts = (place - member + sources) * rows

    keys = kv.shape[0]
    partials = pl.pallas_call(
        da_attend_kernel,
        grid=(CUBE,),
        out_shape=shape_of(CUBE, rows + STAT_ROWS, 4 * HD),
        in_specs=[
            SMEM,
            pl.BlockSpec((1, rows, 2 * HD), lambda i: (i, 0, 0)),
            pl.BlockSpec((keys, 4 * HD), lambda i: (0, 0)),
            pl.BlockSpec((1, keys), lambda i: (0, 0)),
        ],
        out_specs=pl.BlockSpec((1, rows + STAT_ROWS, 4 * HD), lambda i: (i, 0, 0)),
        name="da_attend",
        cost_estimate=pl.CostEstimate(
            flops=8 * CUBE * rows * keys * 2 * HD, bytes_accessed=4 * MIB, transcendentals=0
        ),
        compiler_params=pltpu.CompilerParams(vmem_limit_bytes=48 * MIB),
    )(firsts, queries, kv, places)
    pieces = [partials[0]] + [in_cube(partials[k], count, -k) for k in range(1, CUBE)]

    sw_pieces = [sw_piece] + [in_cube(sw_piece, count, k) for k in range(1, CUBE)]
    sw_query, sw_kv = call(
        functools.partial(sw_project_kernel, rows),
        (shape_of(rows, 2 * HD), shape_of(rows, 2 * HD)),
        [SMEM] + [VMEM] * 7,
        (place_arg, blocks, *sw_pieces, twice(sw_query_gain), twice(sw_key_gain)),
        "sw_project",
        2 * rows * width * sw_cols,
    )
    before = lax.ppermute(
        sw_kv[rows - WINDOW :], "sp", [(z, z + 1) for z in range(count - 1)]
    )
    sw_rows = call(
        sw_attend_kernel,
        shape_of(rows, 2 * HD),
        [SMEM, SMEM] + [VMEM] * 3,
        (place_arg, sink_logit, sw_query, before, sw_kv),
        "sw_attend",
        16 * rows * (rows + WINDOW) * HD,
    )

    da_rows = call(
        merge_kernel,
        shape_of(rows, 2 * HD),
        [SMEM] + [VMEM] * 5,
        (mix_lambda, *pieces, head_gain[None]),
        "merge",
        32 * rows * 2 * HD,
    )

    both = jnp.concatenate([da_rows, sw_rows], axis=1)
    parity = [list(range(c, groups, 2)) for c in range(2)]
    same = lax.all_gather(both, "tp", axis=0, tiled=False, axis_index_groups=parity)
    other = lax.ppermute(same, "tp", [(t, t ^ 1) for t in range(groups)])
    core = lax.rem(lax.axis_index("tp").astype(jnp.int32), 2).reshape(1)
    columns = out_weights.shape[2]
    tile = 512
    return pl.pallas_call(
        mix_kernel,
        grid=(columns // tile,),
        out_shape=shape_of(rows, columns),
        in_specs=[
            SMEM,
            pl.BlockSpec(same.shape, lambda i: (0, 0, 0)),
            pl.BlockSpec(other.shape, lambda i: (0, 0, 0)),
            pl.BlockSpec(out_weights.shape[:2] + (tile,), lambda i: (0, 0, i)),
        ],
        out_specs=pl.BlockSpec((rows, tile), lambda i: (0, i)),
        name="mix",
        cost_estimate=pl.CostEstimate(
            flops=4 * groups * rows * 2 * HD * 2 * columns, bytes_accessed=10 * MIB, transcendentals=0
        ),
        compiler_params=pltpu.CompilerParams(vmem_limit_bytes=48 * MIB),
    )(core, same, other, out_weights)


def solution(mesh):
    return jax.shard_map(
        on_device,
        mesh=mesh,
        in_specs=(
            P(("grp", "sp"), None),
            P(),
            P("sp", "tp"),
            P("sp", "tp"),
            P("sp", "tp"),
            P("sp", "tp"),
            P("sp", "tp"),
            P("sp", "tp"),
            P(),
            P(),
            P(),
            P(),
            P("tp"),
            P(),
            P("tp"),
            P("tp", None),
            P("tp", None),
        ),
        out_specs=P(("grp", "sp"), None),
        check_vma=False,
    )
```

time: 413 us -> 281 us (0.68)
  waiting for transfers between devices: 348 us -> 4.75 us
  blocking collectives: 0 us -> 150 us
  starting transfers between devices: 4.53 us -> 73 us
  matrix products: 21.7 us -> 0 us
  Pallas kernels: 0 us -> 20.1 us
  other arithmetic: 16 us -> 5.96 us
  local copies, waits for them, and re-layouts: 6.75 us -> 11.8 us
    all_gather x3 -> x1, waiting for transfers between devices: 348 us -> 0.01 us  [on_device(): lax.all_gather(jnp.concatenate([da_out_weight, sw_out_weight], axis=0), '...]
    all_gather x0 -> x3, blocking collectives: none -> 150 us  [the longest x1 86.9 us: on_device(): lax.all_gather(shard, 'sp', axis=0, tiled=True, axis_index_groups=strided)]
    ppermute x2 -> x14, starting transfers between devices: 4.4 us -> 73 us  [the longest x12 49.1 us: in_cube(): return lax.ppermute(value, 'sp', pairs)]
    dot_general x14 -> x0, matrix products: 21.7 us -> none  [the longest x6 9.32 us: on_device(): jnp.dot(normed, piece, preferred_element_type=jnp.float32)]
    pallas_call x0 -> x6, Pallas kernels: none -> 20.1 us  [the longest x1 9.24 us: on_device(): pl.pallas_call(da_attend_kernel, grid=(CUBE,), out_shape=shape_of(CUBE, r...]
    reduce_sum x7 -> x1, other arithmetic: 10.8 us -> 1.3 us  [on_device(): mean = jnp.mean(everything * everything, axis=-1, keepdims=True)]
    ppermute x2 -> x14, waiting for transfers between devices: 0.01 us -> 4.7 us  [the longest x12 2.83 us: in_cube(): return lax.ppermute(value, 'sp', pairs)]
  transfers between devices with their start and end apart: 5 -> 15, of which waited for: 3 -> 3; matrix products, arithmetic and copies ran while one was open for 3% -> 5% of each run, Pallas kernels for 0% -> 5%
where the time goes in v1:
time: 281 us; the launch traced here: 280 us
  blocking collectives  150 us (53%)
  starting transfers between devices  73 us (26%)
  Pallas kernels  20.1 us (7%)
  between operations  14.5 us (5%)
  local copies, waits for them, and re-layouts  11.8 us (4%)
  other arithmetic  5.96 us (2%)
  waiting for transfers between devices  4.75 us (2%)
    all_gather x1, blocking collectives, on_device(): lax.all_gather(shard, 'sp', axis=0, tiled=True, axis_index_groups=strided)  86.9 us
    all_gather x1, blocking collectives, on_device(): lax.all_gather(kv_sent, 'sp', axis=0, tiled=True, axis_index_groups=strided)  49.2 us
    ppermute x12, starting transfers between devices, in_cube(): return lax.ppermute(value, 'sp', pairs)  49.1 us
    ppermute x1, starting transfers between devices, on_device(): other = lax.ppermute(same, 'tp', [(t, t ^ 1) for t in range(groups)])  20.8 us
    all_gather x1, blocking collectives, on_device(): lax.all_gather(both, 'tp', axis=0, tiled=False, axis_index_groups=parity)  13.4 us
    pallas_call x1, Pallas kernels, on_device(): pl.pallas_call(da_attend_kernel, grid=(CUBE,), out_shape=shape_of(CUBE, r...  9.24 us
    pallas_call x1, Pallas kernels, on_device(): pl.pallas_call(mix_kernel, grid=(columns // tile,), out_shape=shape_of(ro...  6.32 us
  transfers between devices with their start and end apart: 15, of which 3 were waited for; matrix products, arithmetic and copies ran while one was open for 5% of the time, Pallas kernels for 5%

profile of v1, /device:TPU:33, one launch (start us, length us, event | category | flops | bytes accessed | tf_op | source)
XLA Modules:
  0.0 279.8 jit_solution(430164270390565705)
XLA Ops:
  6.6 2.3 pad_maximum_fusion.1
  9.2 86.9 %all_gather.18 = bf16[512,896]{1,0:T(8,128)(2,1)S(1)} all-gather(bf16[64,896]{1,0:T(8,128)(2,1)S(1)} %concatenate.49), channel_id=1, replica_groups={{0,32,64,96,128,160,192,224},{8,40,72,104,136,168,200,232},{16,48,80,11..., dimensions={0}, use_global_device_ids=true | all-gather | bytes 1032192 | tf_op jit(solution)/shard_map/all_gather | solution.py:228
  96.1 2.0 collective-permute-start
  98.1 6.6 %collective-permute-start.1 = (bf16[512,384]{1,0:T(8,128)(2,1)S(1)}, bf16[512,384]{1,0:T(8,128)(2,1)S(1)}, u32[]{:S(2)}, u32[]{:S(2)}) collective-permute-start(bf16[512,384]{1,0:T(8,128)(2,1)S(1)} %slice.37.w0), channel_id=1, source_target_pairs={{0,16},{8,24},{16,0},{24,8},{32,48},{40,56},{48,32},{56,40},{64,80... | collective-permute-start | bytes 1179656 | tf_op jit(solution)/shard_map/ppermute | solution.py:178
  104.7 2.0 collective-permute-start.2
  107.4 3.1 %collective-permute-start.10 = (bf16[512,256]{1,0:T(8,128)(2,1)S(1)}, bf16[512,256]{1,0:T(8,128)(2,1)S(1)}, u32[]{:S(2)}, u32[]{:S(2)}) collective-permute-start(bf16[512,256]{1,0:T(8,128)(2,1)S(1)} %get-tuple-element.15.w0), channel_id=1, source_target_pairs={{0,16},{8,24},{16,0},{24,8},{32,48},{40,56},{48,32},{56,40},{64,80... | collective-permute-start | bytes 786440 | tf_op jit(solution)/shard_map/ppermute | solution.py:178
  110.5 4.3 %collective-permute-start.11 = (bf16[512,256]{1,0:T(8,128)(2,1)S(1)}, bf16[512,256]{1,0:T(8,128)(2,1)}, u32[]{:S(2)}, u32[]{:S(2)}) collective-permute-start(bf16[512,256]{1,0:T(8,128)(2,1)S(1)} %get-tuple-element.15.w0), channel_id=1, source_target_pairs={{0,24},{8,0},{16,8},{24,16},{32,56},{40,32},{48,40},{56,48},{64,88... | collective-permute-start | bytes 786440 | tf_op jit(solution)/shard_map/ppermute | solution.py:178
  114.8 2.1 concatenate.50
  119.9 2.4 copy.21
  123.7 1.8 fusion
  129.1 2.8 %collective-permute-done.1.w2 = bf16[512,384]{1,0:T(8,128)(2,1)S(1)} collective-permute-done((bf16[512,384]{1,0:T(8,128)(2,1)S(1)}, bf16[512,384]{1,0:T(8,128)(2,1)S(1)}, u32[]{:S(2)}, u32[]{:S(2)}) %collective-permute-start.1) | collective-permute-done | bytes 393248 | tf_op jit(solution)/shard_map/ppermute | solution.py:178
  132.9 13.1 %collective-permute-start.5 = (bf16[256,128]{1,0:T(8,128)(2,1)S(1)}, bf16[256,128]{1,0:T(8,128)(2,1)S(1)}, u32[]{:S(2)}, u32[]{:S(2)}) collective-permute-start(bf16[256,128]{1,0:T(8,128)(2,1)S(1)} %get-tuple-element.10), channel_id=1, source_target_pairs={{0,24},{8,0},{16,8},{24,16},{32,56},{40,32},{48,40},{56,48},{64,88... | collective-permute-start | bytes 196616 | tf_op jit(solution)/shard_map/ppermute | solution.py:178
  146.0 2.4 collective-permute-start.3
  148.3 3.1 %collective-permute-start.4 = (bf16[256,128]{1,0:T(8,128)(2,1)S(1)}, bf16[256,128]{1,0:T(8,128)(2,1)S(1)}, u32[]{:S(2)}, u32[]{:S(2)}) collective-permute-start(bf16[256,128]{1,0:T(8,128)(2,1)S(1)} %get-tuple-element.10), channel_id=1, source_target_pairs={{0,16},{8,24},{16,0},{24,8},{32,48},{40,56},{48,32},{56,40},{64,80... | collective-permute-start | bytes 196616 | tf_op jit(solution)/shard_map/ppermute | solution.py:178
  151.5 49.2 %all_gather.19 = bf16[1984,256]{1,0:T(8,128)(2,1)S(1)} all-gather(bf16[248,256]{1,0:T(8,128)(2,1)S(1)} %get-tuple-element.11), channel_id=1, replica_groups={{0,32,64,96,128,160,192,224},{8,40,72,104,136,168,200,232},{16,48,80,11..., dimensions={0}, use_global_device_ids=true | all-gather | bytes 1142784 | tf_op jit(solution)/shard_map/all_gather | solution.py:257
  200.8 5.4 %collective-permute-start.9 = (bf16[512,256]{1,0:T(8,128)(2,1)S(1)}, bf16[512,256]{1,0:T(8,128)(2,1)S(1)}, u32[]{:S(2)}, u32[]{:S(2)}) collective-permute-start(bf16[512,256]{1,0:T(8,128)(2,1)S(1)} %get-tuple-element.15.w0), channel_id=1, source_target_pairs={{0,8},{8,16},{16,24},{24,0},{32,40},{40,48},{48,56},{56,32},{64,72... | collective-permute-start | bytes 786440 | tf_op jit(solution)/shard_map/ppermute | solution.py:178
  206.2 9.2 %da_attend.1 = bf16[4,272,256]{2,1,0:T(8,128)(2,1)S(1)} custom-call(s32[4]{0:T(128)S(1)} %fusion.3.first_ref, bf16[4,256,128]{2,1,0:T(8,128)(2,1)S(1)} %pad_maximum_fusion.2.q_ref, bf16[2048,256]{1,0:T(8,128)(2,1)S(1)} %pad_maximum_fusion.kv_ref, s32[1,2048]{1,0:T(1,128)S(1)} %add_add_fusion.places_ref), custom_call_target="tpu_custom_call" | custom-call | flops 2147483648 | bytes 4194304 | tf_op jit(solution)/shard_map/da_attend/pallas_call | solution.py:268
  215.6 2.0 collective-permute-start.6
  217.5 3.1 %collective-permute-start.7 = (bf16[272,256]{1,0:T(8,128)(2,1)S(1)}, bf16[272,256]{1,0:T(8,128)(2,1)S(1)}, u32[]{:S(2)}, u32[]{:S(2)}) collective-permute-start(bf16[272,256]{1,0:T(8,128)(2,1)S(1)} %get-tuple-element.18), channel_id=1, source_target_pairs={{0,16},{8,24},{16,0},{24,8},{32,48},{40,56},{48,32},{56,40},{64,80... | collective-permute-start | bytes 417800 | tf_op jit(solution)/shard_map/ppermute | solution.py:178
  220.7 2.2 collective-permute-start.8
  224.6 3.1 %collective-permute-start.12 = (bf16[128,128]{1,0:T(8,128)(2,1)S(1)}, bf16[128,128]{1,0:T(8,128)(2,1)S(1)}, u32[]{:S(2)}, u32[]{:S(2)}) collective-permute-start(bf16[128,128]{1,0:T(8,128)(2,1)S(1)} %slice.35), channel_id=1, source_target_pairs={{0,8},{8,16},{16,24},{24,32},{32,40},{40,48},{48,56},{56,64},{64,7... | collective-permute-start | bytes 98312 | tf_op jit(solution)/shard_map/ppermute | solution.py:296
  230.8 13.4 %all-gather = bf16[1024,256]{1,0:T(8,128)(2,1)S(1)} all-gather(bf16[256,256]{1,0:T(8,128)(2,1)S(1)} %pad_maximum_fusion.3), channel_id=2, replica_groups={{0,2,4,6},{1,3,5,7},{8,10,12,14},{9,11,13,15},{16,18,20,22},{17,19,21,2..., dimensions={0}, use_global_device_ids=true | all-gather | bytes 655360 | tf_op jit(solution)/shard_map/all_gather | solution.py:319
  244.2 20.8 %collective-permute-start.13 = (bf16[4,256,256]{2,1,0:T(8,128)(2,1)S(1)}, bf16[4,256,256]{2,1,0:T(8,128)(2,1)S(1)}, u32[]{:S(2)}, u32[]{:S(2)}) collective-permute-start(bf16[4,256,256]{2,1,0:T(8,128)(2,1)S(1)} %bitcast.29), channel_id=1, source_target_pairs={{0,1},{1,0},{2,3},{3,2},{4,5},{5,4},{6,7},{7,6},{8,9},{9,8},{10,11... | collective-permute-start | bytes 1572872 | tf_op jit(solution)/shard_map/ppermute | solution.py:320
  266.6 6.3 %mix.1 = bf16[256,2048]{1,0:T(8,128)(2,1)} custom-call(s32[1]{0:T(128)} %bitcast.core_ref, bf16[4,256,256]{2,1,0:T(8,128)(2,1)S(1)} %bitcast.30, bf16[4,256,256]{2,1,0:T(8,128)(2,1)S(1)} %collective-permute-done.13.other_ref, bf16[8,256,2048]{2,1,0:T(8,128)(2,1)} %bitcast.38), custom_call_target="tpu_custom_call" | custom-call | flops 4294967296 | bytes 10485760 | tf_op jit(solution)/shard_map/mix/pallas_call | solution.py:324
  (75 shorter events, 15.7 us)
Async XLA Ops:
  6.6 2.5 copy-start.7
  6.6 260.0 %all-gather.4.cloned.1.call-start = ((), (), s32[]{:S(2)}) async-start(), calls=%async_computation | async-start | bytes 9437184 | tf_op jit(solution)/shard_map/all_gather | solution.py:210
  8.9 109.7 %copy-start.2 = (bf16[256,2048]{1,0:T(8,128)(2,1)S(1)}, bf16[256,2048]{1,0:T(8,128)(2,1)}, u32[]{:S(2)}) copy-start(bf16[256,2048]{1,0:T(8,128)(2,1)} %param.17) | copy-start | bytes 3145732
  96.1 26.1 %copy-start.9 = (f32[2048]{0:T(1024)S(1)}, f32[2048]{0:T(1024)}, u32[]{:S(2)}) copy-start(f32[2048]{0:T(1024)} %param.18) | copy-start | bytes 24580
  96.1 33.0 %collective-permute-start = (bf16[512,384]{1,0:T(8,128)(2,1)S(1)}, bf16[512,384]{1,0:T(8,128)(2,1)S(1)}, u32[]{:S(2)}, u32[]{:S(2)}) collective-permute-start(bf16[512,384]{1,0:T(8,128)(2,1)S(1)} %slice.37.w0), channel_id=1, source_target_pairs={{0,8},{8,16},{16,24},{24,0},{32,40},{40,48},{48,56},{56,32},{64,72... | collective-permute-start | bytes 1179656 | tf_op jit(solution)/shard_map/ppermute | solution.py:178
  98.1 33.8 %collective-permute-start.1 = (bf16[512,384]{1,0:T(8,128)(2,1)S(1)}, bf16[512,384]{1,0:T(8,128)(2,1)S(1)}, u32[]{:S(2)}, u32[]{:S(2)}) collective-permute-start(bf16[512,384]{1,0:T(8,128)(2,1)S(1)} %slice.37.w0), channel_id=1, source_target_pairs={{0,16},{8,24},{16,0},{24,8},{32,48},{40,56},{48,32},{56,40},{64,80... | collective-permute-start | bytes 1179656 | tf_op jit(solution)/shard_map/ppermute | solution.py:178
  104.7 27.2 %collective-permute-start.2 = (bf16[512,384]{1,0:T(8,128)(2,1)S(1)}, bf16[512,384]{1,0:T(8,128)(2,1)S(1)}, u32[]{:S(2)}, u32[]{:S(2)}) collective-permute-start(bf16[512,384]{1,0:T(8,128)(2,1)S(1)} %slice.37.w0), channel_id=1, source_target_pairs={{0,24},{8,0},{16,8},{24,16},{32,56},{40,32},{48,40},{56,48},{64,88... | collective-permute-start | bytes 1179656 | tf_op jit(solution)/shard_map/ppermute | solution.py:178
  107.4 113.3 %collective-permute-start.10 = (bf16[512,256]{1,0:T(8,128)(2,1)S(1)}, bf16[512,256]{1,0:T(8,128)(2,1)S(1)}, u32[]{:S(2)}, u32[]{:S(2)}) collective-permute-start(bf16[512,256]{1,0:T(8,128)(2,1)S(1)} %get-tuple-element.15.w0), channel_id=1, source_target_pairs={{0,16},{8,24},{16,0},{24,8},{32,48},{40,56},{48,32},{56,40},{64,80... | collective-permute-start | bytes 786440 | tf_op jit(solution)/shard_map/ppermute | solution.py:178
  110.5 112.5 %collective-permute-start.11 = (bf16[512,256]{1,0:T(8,128)(2,1)S(1)}, bf16[512,256]{1,0:T(8,128)(2,1)}, u32[]{:S(2)}, u32[]{:S(2)}) collective-permute-start(bf16[512,256]{1,0:T(8,128)(2,1)S(1)} %get-tuple-element.15.w0), channel_id=1, source_target_pairs={{0,24},{8,0},{16,8},{24,16},{32,56},{40,32},{48,40},{56,48},{64,88... | collective-permute-start | bytes 786440 | tf_op jit(solution)/shard_map/ppermute | solution.py:178
  125.5 3.4 %copy-start.10 = (f32[64]{0:T(128)S(1)}, f32[64]{0:T(128)}, u32[]{:S(2)}) copy-start(f32[64]{0:T(128)} %param.25) | copy-start | bytes 772
  125.5 3.4 %copy-start.11 = (f32[64]{0:T(128)S(1)}, f32[64]{0:T(128)}, u32[]{:S(2)}) copy-start(f32[64]{0:T(128)} %param.26) | copy-start | bytes 772
  132.9 67.9 %collective-permute-start.5 = (bf16[256,128]{1,0:T(8,128)(2,1)S(1)}, bf16[256,128]{1,0:T(8,128)(2,1)S(1)}, u32[]{:S(2)}, u32[]{:S(2)}) collective-permute-start(bf16[256,128]{1,0:T(8,128)(2,1)S(1)} %get-tuple-element.10), channel_id=1, source_target_pairs={{0,24},{8,0},{16,8},{24,16},{32,56},{40,32},{48,40},{56,48},{64,88... | collective-permute-start | bytes 196616 | tf_op jit(solution)/shard_map/ppermute | solution.py:178
  146.0 60.2 %collective-permute-start.3 = (bf16[256,128]{1,0:T(8,128)(2,1)S(1)}, bf16[256,128]{1,0:T(8,128)(2,1)S(1)}, u32[]{:S(2)}, u32[]{:S(2)}) collective-permute-start(bf16[256,128]{1,0:T(8,128)(2,1)S(1)} %get-tuple-element.10), channel_id=1, source_target_pairs={{0,8},{8,16},{16,24},{24,0},{32,40},{40,48},{48,56},{56,32},{64,72... | collective-permute-start | bytes 196616 | tf_op jit(solution)/shard_map/ppermute | solution.py:178
  148.3 57.8 %collective-permute-start.4 = (bf16[256,128]{1,0:T(8,128)(2,1)S(1)}, bf16[256,128]{1,0:T(8,128)(2,1)S(1)}, u32[]{:S(2)}, u32[]{:S(2)}) collective-permute-start(bf16[256,128]{1,0:T(8,128)(2,1)S(1)} %get-tuple-element.10), channel_id=1, source_target_pairs={{0,16},{8,24},{16,0},{24,8},{32,48},{40,56},{48,32},{56,40},{64,80... | collective-permute-start | bytes 196616 | tf_op jit(solution)/shard_map/ppermute | solution.py:178
  200.8 22.2 %collective-permute-start.9 = (bf16[512,256]{1,0:T(8,128)(2,1)S(1)}, bf16[512,256]{1,0:T(8,128)(2,1)S(1)}, u32[]{:S(2)}, u32[]{:S(2)}) collective-permute-start(bf16[512,256]{1,0:T(8,128)(2,1)S(1)} %get-tuple-element.15.w0), channel_id=1, source_target_pairs={{0,8},{8,16},{16,24},{24,0},{32,40},{40,48},{48,56},{56,32},{64,72... | collective-permute-start | bytes 786440 | tf_op jit(solution)/shard_map/ppermute | solution.py:178
  206.2 16.7 %copy-start.12 = (f32[64]{0:T(128)S(1)}, f32[64]{0:T(128)}, u32[]{:S(2)}) copy-start(f32[64]{0:T(128)} %param.27) | copy-start | bytes 772
  206.2 16.7 %copy-start.13 = (f32[64]{0:T(128)S(1)}, f32[64]{0:T(128)}, u32[]{:S(2)}) copy-start(f32[64]{0:T(128)} %param.28) | copy-start | bytes 772
  215.5 13.2 %copy-start.1 = (f32[2]{0:T(128)S(1)}, f32[2]{0:T(128)}, u32[]{:S(2)}) copy-start(f32[2]{0:T(128)} %sink_ref.1) | copy-start | bytes 28
  215.5 14.6 %copy-start = (f32[128]{0:T(128)S(1)}, f32[128]{0:T(128)}, u32[]{:S(2)}) copy-start(f32[128]{0:T(128)} %param.30) | copy-start | bytes 1540
  215.6 14.5 %collective-permute-start.6 = (bf16[272,256]{1,0:T(8,128)(2,1)S(1)}, bf16[272,256]{1,0:T(8,128)(2,1)S(1)}, u32[]{:S(2)}, u32[]{:S(2)}) collective-permute-start(bf16[272,256]{1,0:T(8,128)(2,1)S(1)} %get-tuple-element.19), channel_id=1, source_target_pairs={{0,24},{8,0},{16,8},{24,16},{32,56},{40,32},{48,40},{56,48},{64,88... | collective-permute-start | bytes 417800 | tf_op jit(solution)/shard_map/ppermute | solution.py:178
  217.5 12.5 %collective-permute-start.7 = (bf16[272,256]{1,0:T(8,128)(2,1)S(1)}, bf16[272,256]{1,0:T(8,128)(2,1)S(1)}, u32[]{:S(2)}, u32[]{:S(2)}) collective-permute-start(bf16[272,256]{1,0:T(8,128)(2,1)S(1)} %get-tuple-element.18), channel_id=1, source_target_pairs={{0,16},{8,24},{16,0},{24,8},{32,48},{40,56},{48,32},{56,40},{64,80... | collective-permute-start | bytes 417800 | tf_op jit(solution)/shard_map/ppermute | solution.py:178
  220.7 9.4 %collective-permute-start.8 = (bf16[272,256]{1,0:T(8,128)(2,1)S(1)}, bf16[272,256]{1,0:T(8,128)(2,1)S(1)}, u32[]{:S(2)}, u32[]{:S(2)}) collective-permute-start(bf16[272,256]{1,0:T(8,128)(2,1)S(1)} %get-tuple-element.17), channel_id=1, source_target_pairs={{0,8},{8,16},{16,24},{24,0},{32,40},{40,48},{48,56},{56,32},{64,72... | collective-permute-start | bytes 417800 | tf_op jit(solution)/shard_map/ppermute | solution.py:178
  224.6 4.1 %collective-permute-start.12 = (bf16[128,128]{1,0:T(8,128)(2,1)S(1)}, bf16[128,128]{1,0:T(8,128)(2,1)S(1)}, u32[]{:S(2)}, u32[]{:S(2)}) collective-permute-start(bf16[128,128]{1,0:T(8,128)(2,1)S(1)} %slice.35), channel_id=1, source_target_pairs={{0,8},{8,16},{16,24},{24,32},{32,40},{40,48},{48,56},{56,64},{64,7... | collective-permute-start | bytes 98312 | tf_op jit(solution)/shard_map/ppermute | solution.py:296
  244.2 22.3 %collective-permute-start.13 = (bf16[4,256,256]{2,1,0:T(8,128)(2,1)S(1)}, bf16[4,256,256]{2,1,0:T(8,128)(2,1)S(1)}, u32[]{:S(2)}, u32[]{:S(2)}) collective-permute-start(bf16[4,256,256]{2,1,0:T(8,128)(2,1)S(1)} %bitcast.29), channel_id=1, source_target_pairs={{0,1},{1,0},{2,3},{3,2},{4,5},{5,4},{6,7},{7,6},{8,9},{9,8},{10,11... | collective-permute-start | bytes 1572872 | tf_op jit(solution)/shard_map/ppermute | solution.py:320
  (6 other events, 15.0 us)
Sparse Core Ops, SparseCore 0:
  9.6 91.7 all-gather.3
